TPU v7x, 32 devices: a whole 2x2x4 slice. The times are simulated.
32 devices in a mesh: ep: 8 (over z, x), tp: 4 (over y, core).
Axes of the slice: x: 2, y: 2, z: 4, core: 2. Of those that a mesh axis runs over, the one named last changes fastest.
Arguments:
- mix_values: bfloat16 [4096, 2048], P('ep', 'tp'), may hold values from -6 to 6
- mix_inner_gate: bfloat16 [4096, 2048], P('ep', 'tp'), may hold values from -6 to 6
- mix_outer_gate: bfloat16 [4096, 2048], P('ep', 'tp'), may hold values from -6 to 6
- conv_taps: bfloat16 [3, 2048], replicated, may hold values from -3 to 3
- mix_out_weight: bfloat16 [2048, 2048], P('tp'), may hold values from -0.125 to 0.125
- moe_input: bfloat16 [4096, 2048], P('ep'), may hold values from -36 to 36
- norm_gain: float32 [2048], replicated, may hold values from 0.1 to 1.9
- routes: int32 [4096, 2], P('ep'), may hold values from 0 to 7, all different within a row; in each aligned block of 128 rows (0 to 127, 128 to 255, ...) at most 64 rows name the same one
- route_weights: float32 [4096, 2], P('ep'), may hold values from 0.05 to 1
- expert_gate: bfloat16 [8, 2048, 1024], P('ep', None, 'tp'), may hold values from -0.125 to 0.125
- expert_up: bfloat16 [8, 2048, 1024], P('ep', None, 'tp'), may hold values from -0.125 to 0.125
- expert_down: bfloat16 [8, 1024, 2048], P('ep', 'tp'), may hold values from -0.1875 to 0.1875
- shared_gate: bfloat16 [2048, 1024], P(None, 'tp'), may hold values from -0.125 to 0.125
- shared_up: bfloat16 [2048, 1024], P(None, 'tp'), may hold values from -0.125 to 0.125
- shared_down: bfloat16 [1024, 2048], P('tp'), may hold values from -0.1875 to 0.1875
Outputs:
- mixed_out: bfloat16 [4096, 2048], P(('ep', 'tp'))
- expert_out: bfloat16 [4096, 2048], P(('ep', 'tp'))
Inputs may be any that keep to these rules, and one draw needn't show every extreme that they name: `routes`: each row names 2 different experts; in each aligned block of 128 rows no expert is named more than 64 times, and in every draw some block names some expert exactly 64 times.
All inputs are finite; a program needn't handle non-finite values.
Results may differ from a plain program's by a relative error of at most 0.012.
Values may be sent and summed in bfloat16 or wider, within the bound.
No kernel may reach another device: no remote copies, remote signals or barrier semaphores. Data moves between devices by JAX's collectives and lax.ppermute only.
A program may use at most 128 MiB of HBM per device.

v0:
```python
import jax
import jax.numpy as jnp
from jax import lax
from jax.sharding import PartitionSpec as P


def from_behind(value, axis, steps):
    count = lax.axis_size(axis)
    initial, last = (max(0, -steps), min(count, count - steps))
    return lax.ppermute(value, axis, [(source, source + steps) for source in range(initial, last)])


def slot_table(route_block, experts, capacity):
    tokens, top = route_block.shape
    flat = route_block.reshape(-1)
    onehot = (flat[:, None] == jnp.arange(experts, dtype=jnp.int32)[None, :]).astype(jnp.int32)
    before = jnp.cumsum(onehot, axis=0) - onehot
    target = flat * capacity + jnp.sum(before * onehot, axis=1)
    match = target[None, :] == jnp.arange(experts * capacity, dtype=jnp.int32)[:, None]
    owner = jnp.sum(
        jnp.where(match, jnp.arange(tokens * top, dtype=jnp.int32)[None, :] // top, 0), axis=1
    )
    filled = jnp.any(match, axis=1)
    return (
        target.reshape(tokens, top),
        owner.reshape(experts, capacity),
        filled.reshape(experts, capacity),
    )


def dispatch(block_rows, owner, filled):
    return jnp.where(filled[:, :, None], block_rows[owner], jnp.zeros((), jnp.bfloat16))


def on_device(
    mix_values,
    mix_inner_gate,
    mix_outer_gate,
    conv_taps,
    mix_out_weight,
    moe_input,
    norm_gain,
    routes,
    route_weights,
    expert_gate,
    expert_up,
    expert_down,
    shared_gate,
    shared_up,
    shared_down,
):
    parts = lax.axis_size("tp")
    member = lax.axis_index("tp")
    groups = lax.axis_size("ep")
    rows_here, width_here = mix_values.shape
    reach = conv_taps.shape[0] - 1
    taps = lax.dynamic_slice_in_dim(conv_taps, member * width_here, width_here, 1).astype(
        jnp.float32
    )
    boundary = from_behind(
        jnp.stack([mix_values[rows_here - reach :], mix_inner_gate[rows_here - reach :]]), "ep", 1
    )
    product = jnp.concatenate(
        [
            boundary[1].astype(jnp.float32) * boundary[0].astype(jnp.float32),
            mix_inner_gate.astype(jnp.float32) * mix_values.astype(jnp.float32),
        ],
        axis=0,
    )
    convolved = taps[0] * product[0:rows_here]
    for offset in range(1, reach + 1):
        convolved = convolved + taps[offset] * product[offset : offset + rows_here]
    gated_rows = (mix_outer_gate.astype(jnp.float32) * convolved).astype(jnp.bfloat16)
    mixed = lax.psum_scatter(
        jnp.dot(gated_rows, mix_out_weight, preferred_element_type=jnp.float32).astype(
            jnp.bfloat16
        ),
        "tp",
        scatter_dimension=0,
        tiled=True,
    )
    local_experts = expert_gate.shape[0]
    experts = local_experts * groups
    width = moe_input.shape[1]
    block = moe_input.shape[0] // parts
    top = routes.shape[1]
    capacity = 2 * block * top // experts
    values = moe_input.astype(jnp.float32)
    scale = lax.rsqrt(jnp.mean(values * values, axis=1, keepdims=True) + 1e-06)
    normed_all = (values * scale * norm_gain).astype(jnp.bfloat16)
    own_weights = lax.dynamic_slice_in_dim(route_weights, member * block, block, 0)
    shared_gate_part = jnp.dot(normed_all, shared_gate, preferred_element_type=jnp.float32)
    shared_up_part = jnp.dot(normed_all, shared_up, preferred_element_type=jnp.float32)
    hidden_shared = (jax.nn.silu(shared_gate_part) * shared_up_part).astype(jnp.bfloat16)
    hidden_shared = hidden_shared.reshape(parts, block, hidden_shared.shape[1])
    own_routes = lax.dynamic_slice_in_dim(routes, member * block, block, 0)
    own_target, owner, filled = slot_table(own_routes, experts, capacity)
    own_rows = lax.dynamic_slice_in_dim(normed_all, member * block, block, 0)
    arrived = lax.all_to_all(
        dispatch(own_rows, owner, filled), "ep", split_axis=0, concat_axis=0, tiled=True
    )
    rows = lax.all_gather(
        arrived.reshape(1, groups, local_experts, capacity, width), "tp", axis=0, tiled=True
    )
    gate_part = jnp.einsum(
        "nsjcd,jdf->nsjcf", rows, expert_gate, preferred_element_type=jnp.float32
    )
    up_part = jnp.einsum("nsjcd,jdf->nsjcf", rows, expert_up, preferred_element_type=jnp.float32)
    hidden_routed = (jax.nn.silu(gate_part) * up_part).astype(jnp.bfloat16)
    routed_rows = groups * local_experts * capacity
    block_span = routed_rows + block
    number = block_span * lax.axis_size("tp") // block_span
    out_routed = jnp.einsum(
        "nsjcf,jfd->nsjcd", hidden_routed, expert_down, preferred_element_type=jnp.float32
    ).reshape(number, routed_rows, width)
    out_shared = jnp.einsum(
        "ntf,fd->ntd", hidden_shared, shared_down, preferred_element_type=jnp.float32
    )
    summed = lax.psum_scatter(
        jnp.concatenate([out_routed, out_shared], axis=1)
        .reshape(block_span * lax.axis_size("tp"), width)
        .astype(jnp.bfloat16),
        "tp",
        scatter_dimension=0,
        tiled=True,
    ).astype(jnp.float32)
    routed_back = (
        summed[:routed_rows].astype(jnp.bfloat16).reshape(groups, local_experts * capacity, width)
    )
    returned = lax.all_to_all(routed_back, "ep", split_axis=0, concat_axis=0, tiled=True).reshape(
        experts * capacity, width
    )
    chosen = returned[own_target]
    mix_weights = 2.5 * own_weights / jnp.sum(own_weights, axis=1, keepdims=True)
    total = summed[routed_rows:]
    for slot_number in range(top):
        total = total + mix_weights[:, slot_number : slot_number + 1] * chosen[
            :, slot_number
        ].astype(jnp.float32)
    expert_out = total.astype(jnp.bfloat16)
    return (mixed, expert_out)


def solution(mesh):
    return jax.shard_map(
        on_device,
        mesh=mesh,
        in_specs=(
            P("ep", "tp"),
            P("ep", "tp"),
            P("ep", "tp"),
            P(),
            P("tp", None),
            P("ep", None),
            P(),
            P("ep", None),
            P("ep", None),
            P("ep", None, "tp"),
            P("ep", None, "tp"),
            P("ep", "tp", None),
            P(None, "tp"),
            P(None, "tp"),
            P("tp", None),
        ),
        out_specs=(P(("ep", "tp"), None), P(("ep", "tp"), None)),
        check_vma=False,
    )
```

profile of v0, /device:TPU:0, one launch (start us, length us, event | category | flops | bytes accessed | tf_op | source)
XLA Modules:
  0.0 325.2 jit_solution(13791687452439275770)
XLA Ops:
  7.2 0.8 constant_dynamic-slice_fusion.2
  9.9 2.2 fusion
  12.7 1.4 copy-done.2
  14.2 3.3 %gather_fusion = bf16[512,2048]{1,0:T(8,128)(2,1)} fusion(bf16[128,2048]{1,0:T(8,128)(2,1)S(1)} %constant_dynamic-slice_fusion.1, s32[1024]{0:T(1024)S(1)} %pad_clamp_fusion.1), kind=kCustom, calls=%fused_computation | custom fusion | bytes 4196352 | tf_op jit(solution)/shard_map/gather | solution.py:32
  17.6 1.8 broadcast_select_fusion
  19.4 55.4 %all_to_all.10 = bf16[8,64,2048]{2,1,0:T(8,128)(2,1)} all-to-all(bf16[8,64,2048]{2,1,0:T(8,128)(2,1)S(1)} %broadcast_select_fusion), channel_id=1, replica_groups=mesh['ep'=8,'tp'=4] {'ep'}, dimensions={0} | all-to-all | bytes 4194304 | tf_op jit(solution)/shard_map/all_to_all | solution.py:99
  75.1 2.7 fusion.39
  79.1 2.0 convolution_convert_fusion.1
  81.1 51.2 %all-gather.3.cloned.1.call-done = bf16[32,64,2048]{2,1,0:T(8,128)(2,1)} async-done(((bf16[8,64,2048]{2,1,0:T(8,128)(2,1)}), bf16[32,64,2048]{2,1,0:T(8,128)(2,1)}) %all-gather.3.cloned.1.call-update) | async-done | bytes 8388624 | tf_op jit(solution)/shard_map/all_gather | solution.py:102
  132.3 7.4 %fusion.22 = f32[4,8,64,256]{3,2,1,0:T(8,128)} fusion(bf16[4,8,64,2048]{3,2,1,0:T(8,128)(2,1)} %bitcast.124, bf16[1,2048,256]{2,1,0:T(8,128)(2,1)} %param.24), kind=kOutput, calls=%fused_computation.39 | convolution fusion | flops 2147483648 | bytes 11534336 | tf_op jit(solution)/shard_map/nsjcd,jdf->nsjcf/dot_general | solution.py:105
  139.6 13.8 %convolution_convert_fusion = bf16[4,8,64,2048]{3,2,1,0:T(8,128)(2,1)} fusion(bf16[1,256,2048]{2,1,0:T(8,128)(2,1)} %param.26, bf16[4,8,64,2048]{3,2,1,0:T(8,128)(2,1)} %bitcast.125, f32[4,8,64,256]{3,2,1,0:T(8,128)} %fusion.22, bf16[1,2048,256]{2,1,0:T(8,128)(2,1)} %param.25), kind=kOutput, calls=%fused_computation.3 | convolution fusion | flops 4302307328 | bytes 20971520 | tf_op jit(solution)/shard_map/nsjcf,jfd->nsjcd/dot_general | solution.py:113
  153.5 12.2 %pad_maximum_fusion = bf16[4,640,2048]{2,1,0:T(8,128)(2,1)} fusion(bf16[4,128,2048]{2,1,0:T(8,128)(2,1)} %convolution_convert_fusion.1, bf16[4,512,2048]{2,1,0:T(8,128)(2,1)} %bitcast.118), kind=kLoop, calls=%fused_computation.2 | loop fusion | flops 20971520 | bytes 20971520 | tf_op jit(solution)/shard_map/concatenate | solution.py:120
  165.7 1.0 copy-done.5
  166.9 3.4 %collective-permute-start = (bf16[2,2,512]{2,1,0:T(2,128)(2,1)S(1)}, bf16[2,2,512]{2,1,0:T(2,128)(2,1)S(1)}, u32[]{:S(2)}, u32[]{:S(2)}) collective-permute-start(bf16[2,2,512]{2,1,0:T(2,128)(2,1)S(1)} %pad_maximum_fusion.2), channel_id=1, source_target_pairs={{0,4},{4,8},{8,12},{12,16},{16,20},{20,24},{24,28},{1,5},{5,9},{9,... | collective-permute-start | bytes 12296 | tf_op jit(solution)/shard_map/ppermute | solution.py:10
  171.0 1.1 convert_multiply_fusion.4
  172.1 78.1 %reduce-scatter.5.cloned.1.call-done = bf16[640,2048]{1,0:T(8,128)(2,1)} async-done(((bf16[2560,2048]{1,0:T(8,128)(2,1)}), bf16[640,2048]{1,0:T(8,128)(2,1)}) %reduce-scatter.5.cloned.1.call-update) | async-done | bytes 2621456 | tf_op jit(solution)/shard_map/reduce_scatter | solution.py:119
  250.2 3.2 slice.86
  253.4 5.6 %all-to-all-start.1 = ((bf16[8,64,2048]{2,1,0:T(8,128)(2,1)}), bf16[8,64,2048]{2,1,0:T(8,128)(2,1)}, u32[]{:S(2)}, u32[]{:S(2)}) async-start(bf16[8,64,2048]{2,1,0:T(8,128)(2,1)} %bitcast.119), calls=%async_computation.3 | async-start | bytes 4194304 | tf_op jit(solution)/shard_map/all_to_all | solution.py:130
  259.4 4.8 %convolution_convert_fusion.2 = bf16[512,2048]{1,0:T(8,128)(2,1)} fusion(bf16[512,2048]{1,0:T(8,128)(2,1)S(1)} %copy-done, f32[2,512]{1,0:T(2,128)S(1)} %multiply_bitcast_fusion, f32[512,512]{1,0:T(8,128)} %convert_multiply_fusion.4, bf16[512,512]{1,0:T(8,128)(2,1)S(1)} %copy-done.10, f32[512]{0:T(512)S(1)} %bitcast.122, f32[512]{0:T(512)S(1)} %bitcast.123, ...), kind=kOutput, calls=%fused_computation.10 | convolution fusion | flops 1077411840 | bytes 5777408 | tf_op jit(solution)/shard_map/dot_general | solution.py:75
  264.9 42.3 %all-to-all-done.1 = bf16[8,64,2048]{2,1,0:T(8,128)(2,1)} async-done(((bf16[8,64,2048]{2,1,0:T(8,128)(2,1)}), bf16[8,64,2048]{2,1,0:T(8,128)(2,1)}, u32[]{:S(2)}, u32[]{:S(2)}) %all-to-all-start.1) | async-done | bytes 2097184 | tf_op jit(solution)/shard_map/all_to_all | solution.py:130
  307.2 5.2 %gather_fusion.1 = bf16[256,2048]{1,0:T(8,128)(2,1)} fusion(bf16[512,2048]{1,0:T(8,128)(2,1)} %bitcast.37, s32[1024]{0:T(1024)S(1)} %pad_clamp_fusion), kind=kCustom, calls=%fused_computation.1 | custom fusion | bytes 2098176 | tf_op jit(solution)/shard_map/gather | solution.py:133
  312.4 1.7 reshape.182
  314.2 1.5 fusion.37
  315.7 3.0 fusion.17
  (61 shorter events, 5.9 us)
Async XLA Ops:
  7.2 252.2 %copy-start = (bf16[512,2048]{1,0:T(8,128)(2,1)S(1)}, bf16[512,2048]{1,0:T(8,128)(2,1)}, u32[]{:S(2)}) copy-start(bf16[512,2048]{1,0:T(8,128)(2,1)} %param.19) | copy-start | bytes 6291460
  7.2 5.0 %copy-start.7 = (f32[2048]{0:T(1024)S(1)}, f32[2048]{0:T(1024)}, u32[]{:S(2)}) copy-start(f32[2048]{0:T(1024)} %param.21) | copy-start | bytes 24580
  7.2 125.1 %all-gather.3.cloned.1.call-start = ((), (), s32[]{:S(2)}) async-start(), calls=%async_computation.6 | async-start | bytes 10485760 | tf_op jit(solution)/shard_map/all_gather | solution.py:102
  9.9 2.3 copy-start.1
  12.7 1.4 copy-start.2
  74.8 175.4 %reduce-scatter.5.cloned.1.call-start = ((), (), s32[]{:S(2)}) async-start(), calls=%async_computation.5 | async-start | bytes 13107200 | tf_op jit(solution)/shard_map/reduce_scatter | solution.py:119
  75.1 2.7 copy-start.3
  75.1 2.8 copy-start.9
  77.9 1.2 copy-start.4
  165.6 1.0 copy-start.5
  165.6 1.2 copy-start.6
  166.9 92.4 %collective-permute-start = (bf16[2,2,512]{2,1,0:T(2,128)(2,1)S(1)}, bf16[2,2,512]{2,1,0:T(2,128)(2,1)S(1)}, u32[]{:S(2)}, u32[]{:S(2)}) collective-permute-start(bf16[2,2,512]{2,1,0:T(2,128)(2,1)S(1)} %pad_maximum_fusion.2), channel_id=1, source_target_pairs={{0,4},{4,8},{8,12},{12,16},{16,20},{20,24},{24,28},{1,5},{5,9},{9,... | collective-permute-start | bytes 12296 | tf_op jit(solution)/shard_map/ppermute | solution.py:10
  253.4 5.9 %copy-start.10 = (bf16[512,512]{1,0:T(8,128)(2,1)S(1)}, bf16[512,512]{1,0:T(8,128)(2,1)}, u32[]{:S(2)}) copy-start(bf16[512,512]{1,0:T(8,128)(2,1)} %param.17) | copy-start | bytes 1572868
  253.4 53.8 %all-to-all-start.1 = ((bf16[8,64,2048]{2,1,0:T(8,128)(2,1)}), bf16[8,64,2048]{2,1,0:T(8,128)(2,1)}, u32[]{:S(2)}, u32[]{:S(2)}) async-start(bf16[8,64,2048]{2,1,0:T(8,128)(2,1)} %bitcast.119), calls=%async_computation.3 | async-start | bytes 4194304 | tf_op jit(solution)/shard_map/all_to_all | solution.py:130
  259.0 59.6 %reduce-scatter.3.cloned.1.call-start = ((), (), s32[]{:S(2)}) async-start(), calls=%async_computation.4 | async-start | bytes 2621440 | tf_op jit(solution)/shard_map/reduce_scatter | solution.py:74
  264.2 0.7 copy-start.8
Sparse Core Ops, SparseCore 0:
  74.9 57.2 all-gather.2
  165.8 84.3 reduce-scatter.4
  264.3 31.3 reduce-scatter.2
where the time goes:
time: 326 us; the launch traced here: 325 us
  waiting for transfers between devices  172 us (53%)
  blocking collectives  55.4 us (17%)
  matrix products  31.4 us (10%)
  other arithmetic  22.7 us (7%)
  local copies, waits for them, and re-layouts  20.4 us (6%)
  between operations  14 us (4%)
  starting transfers between devices  9.53 us (3%)
    reduce_scatter x1, waiting for transfers between devices, on_device(): lax.psum_scatter(jnp.concatenate([out_routed, out_shared], axis=1).reshap...  78.1 us
    all_to_all x1, blocking collectives, on_device(): lax.all_to_all(dispatch(own_rows, owner, filled), 'ep', split_axis=0, con...  55.4 us
    all_gather x1, waiting for transfers between devices, on_device(): lax.all_gather(arrived.reshape(1, groups, local_experts, capacity, width)...  51.2 us
    all_to_all x1, waiting for transfers between devices, on_device(): lax.all_to_all(routed_back, 'ep', split_axis=0, concat_axis=0, tiled=True)  42.3 us
    dot_general x1, matrix products, on_device(): jnp.einsum('nsjcf,jfd->nsjcd', hidden_routed, expert_down, preferred_elem...  13.8 us
    concatenate x1, other arithmetic, on_device(): jnp.concatenate([out_routed, out_shared], axis=1)  12.2 us
    dot_general x1, matrix products, on_device(): jnp.einsum('nsjcd,jdf->nsjcf', rows, expert_gate, preferred_element_type=...  7.36 us
    gather x2, local copies, waits for them, and re-layouts, on_device(): chosen = returned[own_target]  6.94 us
  transfers between devices with their start and end apart: 5, of which 3 were waited for; matrix products, arithmetic and copies ran while one was open for 8% of the time, Pallas kernels for 0%

commit v1 on v0

v1 whole, which is shorter than its diff:
```python
import jax
import jax.numpy as jnp
from jax import lax
from jax.sharding import PartitionSpec as P


def from_behind(value, axis, steps):
    count = lax.axis_size(axis)
    initial, last = (max(0, -steps), min(count, count - steps))
    return lax.ppermute(value, axis, [(source, source + steps) for source in range(initial, last)])


def exchange(value, axis, distance):
    count = lax.axis_size(axis)
    return lax.ppermute(value, axis, [(source, source ^ distance) for source in range(count)])


def distances(axis):
    count = lax.axis_size(axis)
    return [1 << bit for bit in range(count.bit_length() - 1)]


def gather_blocks(value, axis):
    count = lax.axis_size(axis)
    blocks = [value]
    if count & (count - 1):
        for step in range(1, count):
            pairs = [(source, (source + step) % count) for source in range(count)]
            blocks.append(lax.ppermute(value, axis, pairs))
        return blocks
    for distance in reversed(distances(axis)):
        sent = [exchange(value, axis, distance)]
        blocks = blocks + sent + [exchange(held, axis, distance) for held in blocks[1:]]
    return blocks


def add_scatter(partial, axis):
    count = lax.axis_size(axis)
    if count & (count - 1):
        return lax.psum_scatter(partial, axis, scatter_dimension=0, tiled=False).astype(jnp.float32)
    member = lax.axis_index(axis)
    held = partial
    for distance in distances(axis):
        bit = (member // distance) % 2
        pairs = held.reshape(held.shape[0] // 2, 2, *held.shape[1:])
        away = lax.dynamic_index_in_dim(pairs, 1 - bit, 1, keepdims=False)
        kept = lax.dynamic_index_in_dim(pairs, bit, 1, keepdims=False)
        summed = kept.astype(jnp.float32) + exchange(away.astype(jnp.bfloat16), axis, distance).astype(jnp.float32)
        held = summed if held.shape[0] == 2 else summed.astype(jnp.bfloat16)
    return held[0]


def slot_targets(route_block, experts, capacity):
    tokens, top = route_block.shape
    flat = route_block.reshape(-1)
    onehot = (flat[:, None] == jnp.arange(experts, dtype=jnp.int32)[None, :]).astype(jnp.int32)
    before = jnp.cumsum(onehot, axis=0) - onehot
    target = flat * capacity + jnp.sum(before * onehot, axis=1)
    return target.reshape(tokens, top)


def pick(match, rows):
    return jnp.dot(match.astype(jnp.bfloat16), rows, preferred_element_type=jnp.float32)


def on_device(
    mix_values,
    mix_inner_gate,
    mix_outer_gate,
    conv_taps,
    mix_out_weight,
    moe_input,
    norm_gain,
    routes,
    route_weights,
    expert_gate,
    expert_up,
    expert_down,
    shared_gate,
    shared_up,
    shared_down,
):
    parts = lax.axis_size("tp")
    member = lax.axis_index("tp")
    groups = lax.axis_size("ep")
    rows_here, width_here = mix_values.shape
    reach = conv_taps.shape[0] - 1
    all_gate = gather_blocks(expert_gate, "tp")
    all_up = gather_blocks(expert_up, "tp")
    all_down = gather_blocks(expert_down, "tp")
    taps = lax.dynamic_slice_in_dim(conv_taps, member * width_here, width_here, 1).astype(
        jnp.float32
    )
    boundary = from_behind(
        jnp.stack([mix_values[rows_here - reach :], mix_inner_gate[rows_here - reach :]]), "ep", 1
    )
    product = jnp.concatenate(
        [
            boundary[1].astype(jnp.float32) * boundary[0].astype(jnp.float32),
            mix_inner_gate.astype(jnp.float32) * mix_values.astype(jnp.float32),
        ],
        axis=0,
    )
    convolved = taps[0] * product[0:rows_here]
    for offset in range(1, reach + 1):
        convolved = convolved + taps[offset] * product[offset : offset + rows_here]
    gated_rows = (mix_outer_gate.astype(jnp.float32) * convolved).astype(jnp.bfloat16)
    mixed_part = jnp.dot(
        gated_rows, mix_out_weight, preferred_element_type=jnp.float32
    ).astype(jnp.bfloat16)
    local_experts = expert_gate.shape[0]
    experts = local_experts * groups
    width = moe_input.shape[1]
    block = moe_input.shape[0] // parts
    top = routes.shape[1]
    capacity = 2 * block * top // experts
    values = moe_input.astype(jnp.float32)
    scale = lax.rsqrt(jnp.mean(values * values, axis=1, keepdims=True) + 1e-06)
    normed_all = (values * scale * norm_gain).astype(jnp.bfloat16)
    own_weights = lax.dynamic_slice_in_dim(route_weights, member * block, block, 0)
    shared_gate_part = jnp.dot(normed_all, shared_gate, preferred_element_type=jnp.float32)
    shared_up_part = jnp.dot(normed_all, shared_up, preferred_element_type=jnp.float32)
    hidden_shared = (jax.nn.silu(shared_gate_part) * shared_up_part).astype(jnp.bfloat16)
    shared_part = jnp.dot(
        hidden_shared, shared_down, preferred_element_type=jnp.float32
    ).astype(jnp.bfloat16)
    mixed = add_scatter(
        mixed_part.reshape(parts, block, mixed_part.shape[1]), "tp"
    ).astype(jnp.bfloat16)
    shared_own = add_scatter(shared_part.reshape(parts, block, width), "tp")
    own_routes = lax.dynamic_slice_in_dim(routes, member * block, block, 0)
    own_target = slot_targets(own_routes, experts, capacity)
    slots = jnp.arange(experts * capacity, dtype=jnp.int32)
    own_rows = lax.dynamic_slice_in_dim(normed_all, member * block, block, 0)
    holds = own_target[None, :, 0] == slots[:, None]
    for slot_number in range(1, top):
        holds = holds | (own_target[None, :, slot_number] == slots[:, None])
    arrived = lax.all_to_all(
        pick(holds, own_rows).astype(jnp.bfloat16).reshape(experts, capacity, width),
        "ep",
        split_axis=0,
        concat_axis=0,
        tiled=True,
    )
    routed_rows = groups * capacity
    rows = arrived.reshape(groups, local_experts, capacity, width)
    results = []
    for local in range(local_experts):
        mine = rows[:, local].reshape(routed_rows, width)
        hidden = []
        for part in range(parts):
            gate_part = jnp.dot(mine, all_gate[part][local], preferred_element_type=jnp.float32)
            up_part = jnp.dot(mine, all_up[part][local], preferred_element_type=jnp.float32)
            hidden.append((jax.nn.silu(gate_part) * up_part).astype(jnp.bfloat16))
        result = jnp.dot(
            jnp.concatenate(hidden, axis=1),
            jnp.concatenate([held[local] for held in all_down], axis=0),
            preferred_element_type=jnp.float32,
        )
        results.append(result.astype(jnp.bfloat16).reshape(groups, 1, capacity, width))
    routed_back = (results[0] if local_experts == 1 else jnp.concatenate(results, axis=1)).reshape(
        groups, local_experts * capacity, width
    )
    returned = lax.all_to_all(routed_back, "ep", split_axis=0, concat_axis=0, tiled=True).reshape(
        experts * capacity, width
    )
    mix_weights = 2.5 * own_weights / jnp.sum(own_weights, axis=1, keepdims=True)
    total = shared_own
    for slot_number in range(top):
        chosen = pick(own_target[:, slot_number : slot_number + 1] == slots[None, :], returned)
        total = total + mix_weights[:, slot_number : slot_number + 1] * chosen
    expert_out = total.astype(jnp.bfloat16)
    return (mixed, expert_out)


def solution(mesh):
    return jax.shard_map(
        on_device,
        mesh=mesh,
        in_specs=(
            P("ep", "tp"),
            P("ep", "tp"),
            P("ep", "tp"),
            P(),
            P("tp", None),
            P("ep", None),
            P(),
            P("ep", None),
            P("ep", None),
            P("ep", None, "tp"),
            P("ep", None, "tp"),
            P("ep", "tp", None),
            P(None, "tp"),
            P(None, "tp"),
            P("tp", None),
        ),
        out_specs=(P(("ep", "tp"), None), P(("ep", "tp"), None)),
        check_vma=False,
    )
```

time: 326 us -> 165 us (0.51)
  waiting for transfers between devices: 172 us -> 75.6 us
  blocking collectives: 55.4 us -> 0 us
  starting transfers between devices: 9.53 us -> 24.4 us
  between operations: 14 us -> 1.05 us
  local copies, waits for them, and re-layouts: 20.4 us -> 8.46 us
  matrix products: 31.4 us -> 42.5 us
  other arithmetic: 22.7 us -> 12.5 us
    reduce_scatter x2 -> x0, waiting for transfers between devices: 78.1 us -> none  [the longest x1 78.1 us: on_device(): lax.psum_scatter(jnp.concatenate([out_routed, out_shared], axis=1).reshap...]
    all_to_all x1 -> x0, blocking collectives: 55.4 us -> none  [on_device(): lax.all_to_all(dispatch(own_rows, owner, filled), 'ep', split_axis=0, con...]
    all_gather x1 -> x0, waiting for transfers between devices: 51.2 us -> none  [on_device(): lax.all_gather(arrived.reshape(1, groups, local_experts, capacity, width)...]
    ppermute x0 -> x13, waiting for transfers between devices: none -> 51.1 us  [exchange(): lax.ppermute(value, axis, [(source, source ^ distance) for source in rang...]
    all_to_all x1, waiting for transfers between devices: 42.3 us -> 19.2 us  [on_device(): lax.all_to_all(routed_back, 'ep', split_axis=0, concat_axis=0, tiled=True)]
    dot_general x4 -> x13, matrix products: 23.9 us -> 37.3 us  [the longest x4 10.3 us: on_device(): jnp.dot(mine, all_up[part][local], preferred_element_type=jnp.float32)]
    concatenate x1 -> x0, other arithmetic: 12.2 us -> none  [on_device(): jnp.concatenate([out_routed, out_shared], axis=1)]
    gather x3 -> x0, local copies, waits for them, and re-layouts: 10.3 us -> none  [the longest x2 6.94 us: on_device(): chosen = returned[own_target]]
  transfers between devices with their start and end apart: 5 -> 16, of which waited for: 3 -> 6; matrix products, arithmetic and copies ran while one was open for 8% -> 28% of each run, Pallas kernels for 0% -> 0%
where the time goes in v1:
time: 165 us; the launch traced here: 164 us
  waiting for transfers between devices  75.6 us (46%)
  matrix products  42.5 us (26%)
  starting transfers between devices  24.4 us (15%)
  other arithmetic  12.5 us (8%)
  local copies, waits for them, and re-layouts  8.46 us (5%)
    ppermute x13, waiting for transfers between devices, exchange(): lax.ppermute(value, axis, [(source, source ^ distance) for source in rang...  51.1 us
    all_to_all x1, waiting for transfers between devices, on_device(): lax.all_to_all(routed_back, 'ep', split_axis=0, concat_axis=0, tiled=True)  19.2 us
    dot_general x4, matrix products, on_device(): jnp.dot(mine, all_up[part][local], preferred_element_type=jnp.float32)  10.3 us
    dot_general x4, matrix products, on_device(): jnp.dot(mine, all_gate[part][local], preferred_element_type=jnp.float32)  10.3 us
    all_to_all x1, starting transfers between devices, on_device(): lax.all_to_all(pick(holds, own_rows).astype(jnp.bfloat16).reshape(experts...  7.28 us
    ppermute x13, starting transfers between devices, exchange(): lax.ppermute(value, axis, [(source, source ^ distance) for source in rang...  6.95 us
    all_to_all x1, starting transfers between devices, on_device(): lax.all_to_all(routed_back, 'ep', split_axis=0, concat_axis=0, tiled=True)  6.29 us
    dot_general x3, matrix products, pick(): jnp.dot(match.astype(jnp.bfloat16), rows, preferred_element_type=jnp.floa...  6.17 us
  transfers between devices with their start and end apart: 16, of which 6 were waited for; matrix products, arithmetic and copies ran while one was open for 28% of the time, Pallas kernels for 0%

profile of v1, /device:TPU:0, one launch (start us, length us, event | category | flops | bytes accessed | tf_op | source)
XLA Modules:
  0.0 164.5 jit_solution(13920321091130802627)
XLA Ops:
  3.2 2.2 %fusion = f32[512]{0:T(512)S(1)} fusion(bf16[512,2048]{1,0:T(8,128)(2,1)} %param.20), kind=kLoop, calls=%fused_computation.2 | loop fusion | flops 3145216 | bytes 2099200 | tf_op jit(solution)/shard_map/reduce_sum | solution.py:118
  9.3 7.3 %all-to-all-start = ((bf16[8,64,2048]{2,1,0:T(8,128)(2,1)}), bf16[8,64,2048]{2,1,0:T(8,128)(2,1)}, u32[]{:S(2)}, u32[]{:S(2)}) async-start(bf16[8,64,2048]{2,1,0:T(8,128)(2,1)} %bitcast.99), calls=%async_computation | async-start | bytes 4194304 | tf_op jit(solution)/shard_map/all_to_all | solution.py:138
  19.6 3.9 %collective-permute-start = (bf16[2,2,512]{2,1,0:T(2,128)(2,1)S(1)}, bf16[2,2,512]{2,1,0:T(2,128)(2,1)S(1)}, u32[]{:S(2)}, u32[]{:S(2)}) collective-permute-start(bf16[2,2,512]{2,1,0:T(2,128)(2,1)S(1)} %pad_maximum_fusion.1), channel_id=1, source_target_pairs={{0,4},{4,8},{8,12},{12,16},{16,20},{20,24},{24,28},{1,5},{5,9},{9,... | collective-permute-start | bytes 12296 | tf_op jit(solution)/shard_map/ppermute | solution.py:10
  25.8 2.7 %fusion.76 = f32[512,256]{1,0:T(8,128)} fusion(bf16[512,2048]{1,0:T(8,128)(2,1)S(1)} %copy-done.3, bf16[2048,256]{1,0:T(8,128)(2,1)} %param.27), kind=kOutput, calls=%fused_computation.118 | convolution fusion | flops 536870912 | bytes 3670016 | tf_op jit(solution)/shard_map/dot_general | solution.py:121
  28.5 5.3 %collective-permute-done = bf16[2,2,512]{2,1,0:T(2,128)(2,1)S(1)} collective-permute-done((bf16[2,2,512]{2,1,0:T(2,128)(2,1)S(1)}, bf16[2,2,512]{2,1,0:T(2,128)(2,1)S(1)}, u32[]{:S(2)}, u32[]{:S(2)}) %collective-permute-start) | collective-permute-done | bytes 4128 | tf_op jit(solution)/shard_map/ppermute | solution.py:10
  35.3 7.7 %collective-permute-done.5 = bf16[1,2048,256]{2,1,0:T(8,128)(2,1)} collective-permute-done((bf16[1,2048,256]{2,1,0:T(8,128)(2,1)}, bf16[1,2048,256]{2,1,0:T(8,128)(2,1)}, u32[]{:S(2)}, u32[]{:S(2)}) %collective-permute-start.5) | collective-permute-done | bytes 1048608 | tf_op jit(solution)/shard_map/ppermute | solution.py:15
  43.0 22.5 %collective-permute-done.6 = bf16[1,2048,256]{2,1,0:T(8,128)(2,1)} collective-permute-done((bf16[1,2048,256]{2,1,0:T(8,128)(2,1)}, bf16[1,2048,256]{2,1,0:T(8,128)(2,1)}, u32[]{:S(2)}, u32[]{:S(2)}) %collective-permute-start.6) | collective-permute-done | bytes 1048608 | tf_op jit(solution)/shard_map/ppermute | solution.py:15
  65.4 2.6 %fusion.45 = f32[512,256]{1,0:T(8,128)S(1)} fusion(bf16[512,2048]{1,0:T(8,128)(2,1)} %bitcast.18, bf16[1,2048,256]{2,1,0:T(8,128)(2,1)} %param.24), kind=kOutput, calls=%fused_computation.57 | convolution fusion | flops 536870912 | bytes 3670016 | tf_op jit(solution)/shard_map/dot_general | solution.py:152
  68.0 2.6 %fusion.17 = bf16[512,256]{1,0:T(8,128)(2,1)S(1)} fusion(bf16[512,2048]{1,0:T(8,128)(2,1)} %bitcast.18, bf16[1,2048,256]{2,1,0:T(8,128)(2,1)} %param.25, f32[512,256]{1,0:T(8,128)S(1)} %fusion.45), kind=kOutput, calls=%fused_computation.26 | convolution fusion | flops 537657344 | bytes 3932160 | tf_op jit(solution)/shard_map/dot_general | solution.py:153
  70.6 2.6 %fusion.42 = f32[512,256]{1,0:T(8,128)S(1)} fusion(bf16[512,2048]{1,0:T(8,128)(2,1)} %bitcast.18, bf16[1,2048,256]{2,1,0:T(8,128)(2,1)} %collective-permute-done.5), kind=kOutput, calls=%fused_computation.54 | convolution fusion | flops 536870912 | bytes 3670016 | tf_op jit(solution)/shard_map/dot_general | solution.py:152
  73.2 2.7 %multiply_convert_fusion.2 = bf16[512,256]{1,0:T(8,128)(2,1)S(1)} fusion(f32[512,256]{1,0:T(8,128)S(1)} %fusion.42, bf16[512,2048]{1,0:T(8,128)(2,1)} %bitcast.18, bf16[1,2048,256]{2,1,0:T(8,128)(2,1)} %collective-permute-done.6), kind=kOutput, calls=%fused_computation.69 | convolution fusion | flops 537657344 | bytes 3932160 | tf_op jit(solution)/shard_map/dot_general | solution.py:153
  75.8 10.7 %collective-permute-done.11 = bf16[1,256,2048]{2,1,0:T(8,128)(2,1)} collective-permute-done((bf16[1,256,2048]{2,1,0:T(8,128)(2,1)}, bf16[1,256,2048]{2,1,0:T(8,128)(2,1)}, u32[]{:S(2)}, u32[]{:S(2)}) %collective-permute-start.11) | collective-permute-done | bytes 1048608 | tf_op jit(solution)/shard_map/ppermute | solution.py:15
  87.0 2.6 %fusion.34 = f32[512,256]{1,0:T(8,128)S(1)} fusion(bf16[512,2048]{1,0:T(8,128)(2,1)} %bitcast.18, bf16[1,2048,256]{2,1,0:T(8,128)(2,1)} %collective-permute-done.9), kind=kOutput, calls=%fused_computation.46 | convolution fusion | flops 536870912 | bytes 3670016 | tf_op jit(solution)/shard_map/dot_general | solution.py:152
  89.6 2.6 %fusion.38 = f32[512,256]{1,0:T(8,128)S(1)} fusion(bf16[512,2048]{1,0:T(8,128)(2,1)} %bitcast.18, bf16[1,2048,256]{2,1,0:T(8,128)(2,1)} %collective-permute-done.7), kind=kOutput, calls=%fused_computation.50 | convolution fusion | flops 536870912 | bytes 3670016 | tf_op jit(solution)/shard_map/dot_general | solution.py:152
  92.2 2.6 %multiply_convert_fusion = bf16[512,256]{1,0:T(8,128)(2,1)S(1)} fusion(f32[512,256]{1,0:T(8,128)S(1)} %fusion.34, bf16[512,2048]{1,0:T(8,128)(2,1)} %bitcast.18, bf16[1,2048,256]{2,1,0:T(8,128)(2,1)} %collective-permute-done.10), kind=kOutput, calls=%fused_computation.67 | convolution fusion | flops 537657344 | bytes 3932160 | tf_op jit(solution)/shard_map/dot_general | solution.py:153
  94.8 2.6 %multiply_convert_fusion.1 = bf16[512,256]{1,0:T(8,128)(2,1)S(1)} fusion(f32[512,256]{1,0:T(8,128)S(1)} %fusion.38, bf16[512,2048]{1,0:T(8,128)(2,1)} %bitcast.18, bf16[1,2048,256]{2,1,0:T(8,128)(2,1)} %collective-permute-done.8), kind=kOutput, calls=%fused_computation.68 | convolution fusion | flops 537657344 | bytes 3932160 | tf_op jit(solution)/shard_map/dot_general | solution.py:153
  97.4 4.9 %fusion.11 = bf16[512,2048]{1,0:T(8,128)(2,1)} fusion(bf16[256,2048]{1,0:T(8,128)(2,1)S(1)} %bitcast.110, bf16[256,2048]{1,0:T(8,128)(2,1)S(1)} %bitcast.109, bf16[256,2048]{1,0:T(8,128)(2,1)} %bitcast.28, bf16[256,2048]{1,0:T(8,128)(2,1)S(1)} %bitcast.108, bf16[512,256]{1,0:T(8,128)(2,1)S(1)} %multiply_convert_fusion, ...), kind=kOutput, calls=%fused_computation.14 | convolution fusion | flops 2169503744 | bytes 7340032 | tf_op jit(solution)/shard_map/dot_general | solution.py:155
  102.2 6.3 %all-to-all-start.1 = ((bf16[8,64,2048]{2,1,0:T(8,128)(2,1)}), bf16[8,64,2048]{2,1,0:T(8,128)(2,1)}, u32[]{:S(2)}, u32[]{:S(2)}) async-start(bf16[8,64,2048]{2,1,0:T(8,128)(2,1)} %bitcast.104), calls=%async_computation.1 | async-start | bytes 4194304 | tf_op jit(solution)/shard_map/all_to_all | solution.py:164
  108.5 2.5 %convolution_convert_fusion.2 = bf16[512,2048]{1,0:T(8,128)(2,1)S(1)} fusion(bf16[512,2048]{1,0:T(8,128)(2,1)S(1)} %copy-done, f32[2,512]{1,0:T(2,128)S(1)} %multiply_bitcast_fusion, f32[512,512]{1,0:T(8,128)S(1)} %convert_multiply_fusion.2, bf16[512,512]{1,0:T(8,128)(2,1)} %param.17, f32[512]{0:T(512)S(1)} %bitcast.106, f32[512]{0:T(512)S(1)} %bitcast.107, ...), kind=kOutput, calls=%fused_computation.16 | convolution fusion | flops 1077411840 | bytes 5777408 | tf_op jit(solution)/shard_map/dot_general | solution.py:108
  113.4 5.7 %convolution_convert_fusion = bf16[512,2048]{1,0:T(8,128)(2,1)} fusion(bf16[256,2048]{1,0:T(8,128)(2,1)S(1)} %copy-done.9, bf16[512,2048]{1,0:T(8,128)(2,1)} %copy-done.2, bf16[2048,256]{1,0:T(8,128)(2,1)} %param.28, f32[512,256]{1,0:T(8,128)} %fusion.76), kind=kOutput, calls=%fused_computation.13 | convolution fusion | flops 1075576832 | bytes 6815744 | tf_op jit(solution)/shard_map/dot_general | solution.py:124
  121.1 2.1 %fusion.15 = bf16[2,128,2048]{2,1,0:T(8,128)(2,1)S(1)} fusion(bf16[2,128,2048]{2,1,0:T(8,128)(2,1)} %collective-permute-done.1, bf16[2,2,128,2048]{3,2,1,0:T(8,128)(2,1)} %bitcast.103, s32[]{:T(128)S(6)} %select_n.50), kind=kLoop, calls=%fused_computation.22 | loop fusion | flops 2097152 | bytes 3145732 | tf_op jit(solution)/shard_map/convert_element_type | solution.py:49
  127.8 10.3 %collective-permute-done.2 = bf16[1,128,2048]{2,1,0:T(8,128)(2,1)S(1)} collective-permute-done((bf16[1,128,2048]{2,1,0:T(8,128)(2,1)S(1)}, bf16[1,128,2048]{2,1,0:T(8,128)(2,1)S(1)}, u32[]{:S(2)}, u32[]{:S(2)}) %collective-permute-start.2) | collective-permute-done | bytes 524320 | tf_op jit(solution)/shard_map/ppermute | solution.py:15
  139.0 19.2 %all-to-all-done.1 = bf16[8,64,2048]{2,1,0:T(8,128)(2,1)} async-done(((bf16[8,64,2048]{2,1,0:T(8,128)(2,1)}), bf16[8,64,2048]{2,1,0:T(8,128)(2,1)}, u32[]{:S(2)}, u32[]{:S(2)}) %all-to-all-start.1) | async-done | bytes 2097184 | tf_op jit(solution)/shard_map/all_to_all | solution.py:164
  162.4 2.1 %fusion.48 = bf16[128,2048]{1,0:T(8,128)(2,1)} fusion(f32[128,2048]{1,0:T(8,128)S(1)} %convolution_multiply_fusion, f32[128,2048]{1,0:T(8,128)S(1)} %convolution_multiply_fusion.1, bf16[1,128,2048]{2,1,0:T(8,128)(2,1)} %collective-permute-done.4, bf16[2,128,2048]{2,1,0:T(8,128)(2,1)S(1)} %fusion.14, s32[]{:T(128)S(6)} %select_n.54), kind=kLoop, calls=%fused_computation.61 | loop fusion | flops 1572864 | bytes 3670020 | tf_op jit(solution)/shard_map/convert_element_type | solution.py:172
  (76 shorter events, 27.7 us)
Async XLA Ops:
  0.6 107.9 %copy-start = (bf16[512,2048]{1,0:T(8,128)(2,1)S(1)}, bf16[512,2048]{1,0:T(8,128)(2,1)}, u32[]{:S(2)}) copy-start(bf16[512,2048]{1,0:T(8,128)(2,1)} %param.19) | copy-start | bytes 6291460
  0.6 4.8 %copy-start.6 = (f32[2048]{0:T(1024)S(1)}, f32[2048]{0:T(1024)}, u32[]{:S(2)}) copy-start(f32[2048]{0:T(1024)} %param.21) | copy-start | bytes 24580
  3.0 2.4 %copy-start.1 = (bf16[512,2048]{1,0:T(8,128)(2,1)S(1)}, bf16[512,2048]{1,0:T(8,128)(2,1)}, u32[]{:S(2)}) copy-start(bf16[512,2048]{1,0:T(8,128)(2,1)} %param.20) | copy-start | bytes 6291460
  9.3 56.1 %all-to-all-start = ((bf16[8,64,2048]{2,1,0:T(8,128)(2,1)}), bf16[8,64,2048]{2,1,0:T(8,128)(2,1)}, u32[]{:S(2)}, u32[]{:S(2)}) async-start(bf16[8,64,2048]{2,1,0:T(8,128)(2,1)} %bitcast.99), calls=%async_computation | async-start | bytes 4194304 | tf_op jit(solution)/shard_map/all_to_all | solution.py:138
  16.6 26.3 %collective-permute-start.5 = (bf16[1,2048,256]{2,1,0:T(8,128)(2,1)}, bf16[1,2048,256]{2,1,0:T(8,128)(2,1)}, u32[]{:S(2)}, u32[]{:S(2)}) collective-permute-start(bf16[1,2048,256]{2,1,0:T(8,128)(2,1)} %param.24), channel_id=1, source_target_pairs={{0,2},{1,3},{2,0},{3,1},{4,6},{5,7},{6,4},{7,5},{8,10},{9,11},{10,... | collective-permute-start | bytes 3145736 | tf_op jit(solution)/shard_map/ppermute | solution.py:15
  18.1 71.4 %collective-permute-start.7 = (bf16[1,2048,256]{2,1,0:T(8,128)(2,1)}, bf16[1,2048,256]{2,1,0:T(8,128)(2,1)}, u32[]{:S(2)}, u32[]{:S(2)}) collective-permute-start(bf16[1,2048,256]{2,1,0:T(8,128)(2,1)} %param.24), channel_id=1, source_target_pairs={{0,1},{1,0},{2,3},{3,2},{4,5},{5,4},{6,7},{7,6},{8,9},{9,8},{10,11... | collective-permute-start | bytes 3145736 | tf_op jit(solution)/shard_map/ppermute | solution.py:15
  18.1 47.3 %collective-permute-start.6 = (bf16[1,2048,256]{2,1,0:T(8,128)(2,1)}, bf16[1,2048,256]{2,1,0:T(8,128)(2,1)}, u32[]{:S(2)}, u32[]{:S(2)}) collective-permute-start(bf16[1,2048,256]{2,1,0:T(8,128)(2,1)} %param.25), channel_id=1, source_target_pairs={{0,2},{1,3},{2,0},{3,1},{4,6},{5,7},{6,4},{7,5},{8,10},{9,11},{10,... | collective-permute-start | bytes 3145736 | tf_op jit(solution)/shard_map/ppermute | solution.py:15
  18.7 76.1 %collective-permute-start.8 = (bf16[1,2048,256]{2,1,0:T(8,128)(2,1)}, bf16[1,2048,256]{2,1,0:T(8,128)(2,1)}, u32[]{:S(2)}, u32[]{:S(2)}) collective-permute-start(bf16[1,2048,256]{2,1,0:T(8,128)(2,1)} %param.25), channel_id=1, source_target_pairs={{0,1},{1,0},{2,3},{3,2},{4,5},{5,4},{6,7},{7,6},{8,9},{9,8},{10,11... | collective-permute-start | bytes 3145736 | tf_op jit(solution)/shard_map/ppermute | solution.py:15
  19.6 14.2 %collective-permute-start = (bf16[2,2,512]{2,1,0:T(2,128)(2,1)S(1)}, bf16[2,2,512]{2,1,0:T(2,128)(2,1)S(1)}, u32[]{:S(2)}, u32[]{:S(2)}) collective-permute-start(bf16[2,2,512]{2,1,0:T(2,128)(2,1)S(1)} %pad_maximum_fusion.1), channel_id=1, source_target_pairs={{0,4},{4,8},{8,12},{12,16},{16,20},{20,24},{24,28},{1,5},{5,9},{9,... | collective-permute-start | bytes 12296 | tf_op jit(solution)/shard_map/ppermute | solution.py:10
  23.6 2.2 %copy-start.3 = (bf16[512,2048]{1,0:T(8,128)(2,1)S(1)}, bf16[512,2048]{1,0:T(8,128)(2,1)}, u32[]{:S(2)}) copy-start(bf16[512,2048]{1,0:T(8,128)(2,1)} %copy-done.2) | copy-start | bytes 6291460
  33.8 52.7 %collective-permute-start.11 = (bf16[1,256,2048]{2,1,0:T(8,128)(2,1)}, bf16[1,256,2048]{2,1,0:T(8,128)(2,1)}, u32[]{:S(2)}, u32[]{:S(2)}) collective-permute-start(bf16[1,256,2048]{2,1,0:T(8,128)(2,1)} %param.26), channel_id=1, source_target_pairs={{0,2},{1,3},{2,0},{3,1},{4,6},{5,7},{6,4},{7,5},{8,10},{9,11},{10,... | collective-permute-start | bytes 3145736 | tf_op jit(solution)/shard_map/ppermute | solution.py:15
  43.0 43.5 %collective-permute-start.9 = (bf16[1,2048,256]{2,1,0:T(8,128)(2,1)}, bf16[1,2048,256]{2,1,0:T(8,128)(2,1)}, u32[]{:S(2)}, u32[]{:S(2)}) collective-permute-start(bf16[1,2048,256]{2,1,0:T(8,128)(2,1)} %collective-permute-done.5), channel_id=1, source_target_pairs={{0,1},{1,0},{2,3},{3,2},{4,5},{5,4},{6,7},{7,6},{8,9},{9,8},{10,11... | collective-permute-start | bytes 3145736 | tf_op jit(solution)/shard_map/ppermute | solution.py:15
  65.4 26.7 %collective-permute-start.10 = (bf16[1,2048,256]{2,1,0:T(8,128)(2,1)}, bf16[1,2048,256]{2,1,0:T(8,128)(2,1)}, u32[]{:S(2)}, u32[]{:S(2)}) collective-permute-start(bf16[1,2048,256]{2,1,0:T(8,128)(2,1)} %collective-permute-done.6), channel_id=1, source_target_pairs={{0,1},{1,0},{2,3},{3,2},{4,5},{5,4},{6,7},{7,6},{8,9},{9,8},{10,11... | collective-permute-start | bytes 3145736 | tf_op jit(solution)/shard_map/ppermute | solution.py:15
  73.2 13.3 %copy-start.8 = (bf16[1,256,2048]{2,1,0:T(8,128)(2,1)S(1)}, bf16[1,256,2048]{2,1,0:T(8,128)(2,1)}, u32[]{:S(2)}) copy-start(bf16[1,256,2048]{2,1,0:T(8,128)(2,1)} %param.26) | copy-start | bytes 3145732
  86.5 10.8 %collective-permute-start.12 = (bf16[1,256,2048]{2,1,0:T(8,128)(2,1)S(1)}, bf16[1,256,2048]{2,1,0:T(8,128)(2,1)S(1)}, u32[]{:S(2)}, u32[]{:S(2)}) collective-permute-start(bf16[1,256,2048]{2,1,0:T(8,128)(2,1)S(1)} %copy-done.8), channel_id=1, source_target_pairs={{0,1},{1,0},{2,3},{3,2},{4,5},{5,4},{6,7},{7,6},{8,9},{9,8},{10,11... | collective-permute-start | bytes 3145736 | tf_op jit(solution)/shard_map/ppermute | solution.py:15
  86.5 10.8 %collective-permute-start.13 = (bf16[1,256,2048]{2,1,0:T(8,128)(2,1)}, bf16[1,256,2048]{2,1,0:T(8,128)(2,1)S(1)}, u32[]{:S(2)}, u32[]{:S(2)}) collective-permute-start(bf16[1,256,2048]{2,1,0:T(8,128)(2,1)} %collective-permute-done.11), channel_id=1, source_target_pairs={{0,1},{1,0},{2,3},{3,2},{4,5},{5,4},{6,7},{7,6},{8,9},{9,8},{10,11... | collective-permute-start | bytes 3145736 | tf_op jit(solution)/shard_map/ppermute | solution.py:15
  102.2 56.0 %all-to-all-start.1 = ((bf16[8,64,2048]{2,1,0:T(8,128)(2,1)}), bf16[8,64,2048]{2,1,0:T(8,128)(2,1)}, u32[]{:S(2)}, u32[]{:S(2)}) async-start(bf16[8,64,2048]{2,1,0:T(8,128)(2,1)} %bitcast.104), calls=%async_computation.1 | async-start | bytes 4194304 | tf_op jit(solution)/shard_map/all_to_all | solution.py:164
  111.0 2.4 %copy-start.9 = (bf16[256,2048]{1,0:T(8,128)(2,1)S(1)}, bf16[256,2048]{1,0:T(8,128)(2,1)}, u32[]{:S(2)}) copy-start(bf16[256,2048]{1,0:T(8,128)(2,1)} %param.29) | copy-start | bytes 3145732
  113.4 7.7 %collective-permute-start.1 = (bf16[2,128,2048]{2,1,0:T(8,128)(2,1)}, bf16[2,128,2048]{2,1,0:T(8,128)(2,1)}, u32[]{:S(2)}, u32[]{:S(2)}) collective-permute-start(bf16[2,128,2048]{2,1,0:T(8,128)(2,1)} %dynamic-slice_bitcast_fusion.1), channel_id=1, source_target_pairs={{0,1},{1,0},{2,3},{3,2},{4,5},{5,4},{6,7},{7,6},{8,9},{9,8},{10,11... | collective-permute-start | bytes 3145736 | tf_op jit(solution)/shard_map/ppermute | solution.py:15
  119.1 1.9 %copy-start.7 = (f32[512,2]{0,1:T(2,128)S(1)}, f32[512,2]{0,1:T(2,128)}, u32[]{:S(2)}) copy-start(f32[512,2]{0,1:T(2,128)} %param.23) | copy-start | bytes 12292
  120.4 4.4 %collective-permute-start.3 = (bf16[2,128,2048]{2,1,0:T(8,128)(2,1)S(1)}, bf16[2,128,2048]{2,1,0:T(8,128)(2,1)}, u32[]{:S(2)}, u32[]{:S(2)}) collective-permute-start(bf16[2,128,2048]{2,1,0:T(8,128)(2,1)S(1)} %dynamic-slice_bitcast_fusion), channel_id=1, source_target_pairs={{0,1},{1,0},{2,3},{3,2},{4,5},{5,4},{6,7},{7,6},{8,9},{9,8},{10,11... | collective-permute-start | bytes 3145736 | tf_op jit(solution)/shard_map/ppermute | solution.py:15
  121.1 3.8 %copy-start.4 = (bf16[512,2048]{1,0:T(8,128)(2,1)S(1)}, bf16[512,2048]{1,0:T(8,128)(2,1)}, u32[]{:S(2)}) copy-start(bf16[512,2048]{1,0:T(8,128)(2,1)} %convolution_convert_fusion) | copy-start | bytes 6291460
  123.2 14.9 %collective-permute-start.2 = (bf16[1,128,2048]{2,1,0:T(8,128)(2,1)S(1)}, bf16[1,128,2048]{2,1,0:T(8,128)(2,1)S(1)}, u32[]{:S(2)}, u32[]{:S(2)}) collective-permute-start(bf16[1,128,2048]{2,1,0:T(8,128)(2,1)S(1)} %constant_dynamic-slice_fusion.3), channel_id=1, source_target_pairs={{0,2},{1,3},{2,0},{3,1},{4,6},{5,7},{6,4},{7,5},{8,10},{9,11},{10,... | collective-permute-start | bytes 1572872 | tf_op jit(solution)/shard_map/ppermute | solution.py:15
  127.3 35.1 %collective-permute-start.4 = (bf16[1,128,2048]{2,1,0:T(8,128)(2,1)}, bf16[1,128,2048]{2,1,0:T(8,128)(2,1)}, u32[]{:S(2)}, u32[]{:S(2)}) collective-permute-start(bf16[1,128,2048]{2,1,0:T(8,128)(2,1)} %constant_dynamic-slice_fusion.2), channel_id=1, source_target_pairs={{0,2},{1,3},{2,0},{3,1},{4,6},{5,7},{6,4},{7,5},{8,10},{9,11},{10,... | collective-permute-start | bytes 1572872 | tf_op jit(solution)/shard_map/ppermute | solution.py:15
  (2 other events, 2.7 us)

commit v2 on v1

--- a/solution.py
+++ b/solution.py
@@ -1,6 +1,8 @@
 import jax
 import jax.numpy as jnp
 from jax import lax
+from jax.experimental import pallas as pl
+from jax.experimental.pallas import tpu as pltpu
 from jax.sharding import PartitionSpec as P
 
 
@@ -61,6 +63,28 @@
 
 def pick(match, rows):
     return jnp.dot(match.astype(jnp.bfloat16), rows, preferred_element_type=jnp.float32)
+
+
+def expert_body(*refs):
+    rows, out = refs[0], refs[-1]
+    parts = (len(refs) - 2) // 3
+    gates, ups, downs = refs[1 : 1 + parts], refs[1 + parts : 1 + 2 * parts], refs[1 + 2 * parts : -1]
+    total = None
+    for gate, up, down in zip(gates, ups, downs):
+        gate_part = jnp.dot(rows[...], gate[...], preferred_element_type=jnp.float32)
+        up_part = jnp.dot(rows[...], up[...], preferred_element_type=jnp.float32)
+        hidden = (gate_part / (1.0 + jnp.exp(-gate_part)) * up_part).astype(jnp.bfloat16)
+        result = jnp.dot(hidden, down[...], preferred_element_type=jnp.float32)
+        total = result if total is None else total + result
+    out[...] = total.astype(jnp.bfloat16)
+
+
+def run_expert(rows, gates, ups, downs):
+    return pl.pallas_call(
+        expert_body,
+        out_shape=jax.ShapeDtypeStruct((rows.shape[0], downs[0].shape[1]), jnp.bfloat16),
+        compiler_params=pltpu.CompilerParams(vmem_limit_bytes=56 * 1024 * 1024),
+    )(rows, *gates, *ups, *downs)
 
 
 def on_device(
@@ -147,17 +171,13 @@
     results = []
     for local in range(local_experts):
         mine = rows[:, local].reshape(routed_rows, width)
-        hidden = []
-        for part in range(parts):
-            gate_part = jnp.dot(mine, all_gate[part][local], preferred_element_type=jnp.float32)
-            up_part = jnp.dot(mine, all_up[part][local], preferred_element_type=jnp.float32)
-            hidden.append((jax.nn.silu(gate_part) * up_part).astype(jnp.bfloat16))
-        result = jnp.dot(
-            jnp.concatenate(hidden, axis=1),
-            jnp.concatenate([held[local] for held in all_down], axis=0),
-            preferred_element_type=jnp.float32,
+        result = run_expert(
+            mine,
+            [held[local] for held in all_gate],
+            [held[local] for held in all_up],
+            [held[local] for held in all_down],
         )
-        results.append(result.astype(jnp.bfloat16).reshape(groups, 1, capacity, width))
+        results.append(result.reshape(groups, 1, capacity, width))
     routed_back = (results[0] if local_experts == 1 else jnp.concatenate(results, axis=1)).reshape(
         groups, local_experts * capacity, width
     )

time: 165 us -> 170 us (1.030)
  matrix products: 42.5 us -> 17 us
  waiting for transfers between devices: 75.6 us -> 89.8 us
  Pallas kernels: 0 us -> 13.2 us
  other arithmetic: 12.5 us -> 14.9 us
    dot_general x9 -> x0, matrix products: 25.5 us -> none  [the longest x4 10.3 us: on_device(): jnp.dot(mine, all_up[part][local], preferred_element_type=jnp.float32)]
    pallas_call x0 -> x1, Pallas kernels: none -> 13.2 us  [run_expert(): pl.pallas_call(expert_body, out_shape=jax.ShapeDtypeStruct((rows.shape[0]...]
    ppermute x13, waiting for transfers between devices: 51.1 us -> 62.9 us  [exchange(): lax.ppermute(value, axis, [(source, source ^ distance) for source in rang...]
    ppermute x1, waiting for transfers between devices: 5.28 us -> 8.93 us  [from_behind(): lax.ppermute(value, axis, [(source, source + steps) for source in range(i...]
    unnamed x21 -> x23, local copies, waits for them, and re-layouts: 2.83 us -> 3.77 us
  transfers between devices with their start and end apart: 16 -> 16, of which waited for: 6 -> 6; matrix products, arithmetic and copies ran while one was open for 28% -> 16% of each run, Pallas kernels for 0% -> 0%
where the time goes in v2:
time: 170 us; the launch traced here: 169 us
  waiting for transfers between devices  89.8 us (53%)
  starting transfers between devices  23.8 us (14%)
  matrix products  17 us (10%)
  other arithmetic  14.9 us (9%)
  Pallas kernels  13.2 us (8%)
  local copies, waits for them, and re-layouts  9.41 us (6%)
    ppermute x13, waiting for transfers between devices, exchange(): lax.ppermute(value, axis, [(source, source ^ distance) for source in rang...  62.9 us
    all_to_all x1, waiting for transfers between devices, on_device(): lax.all_to_all(routed_back, 'ep', split_axis=0, concat_axis=0, tiled=True)  18 us
    pallas_call x1, Pallas kernels, run_expert(): pl.pallas_call(expert_body, out_shape=jax.ShapeDtypeStruct((rows.shape[0]...  13.2 us
    ppermute x1, waiting for transfers between devices, from_behind(): lax.ppermute(value, axis, [(source, source + steps) for source in range(i...  8.93 us
    all_to_all x1, starting transfers between devices, on_device(): lax.all_to_all(pick(holds, own_rows).astype(jnp.bfloat16).reshape(experts...  7.41 us
    ppermute x13, starting transfers between devices, exchange(): lax.ppermute(value, axis, [(source, source ^ distance) for source in rang...  6.8 us
    dot_general x3, matrix products, pick(): jnp.dot(match.astype(jnp.bfloat16), rows, preferred_element_type=jnp.floa...  6.16 us
    all_to_all x1, starting transfers between devices, on_device(): lax.all_to_all(routed_back, 'ep', split_axis=0, concat_axis=0, tiled=True)  5.78 us
  transfers between devices with their start and end apart: 16, of which 6 were waited for; matrix products, arithmetic and copies ran while one was open for 16% of the time, Pallas kernels for 0%

profile of v2, /device:TPU:0, one launch (start us, length us, event | category | flops | bytes accessed | tf_op | source)
XLA Modules:
  0.0 169.2 jit_solution(10206978198907750930)
XLA Ops:
  1.9 2.1 %fusion = f32[512]{0:T(512)S(1)} fusion(bf16[512,2048]{1,0:T(8,128)(2,1)} %param.20), kind=kLoop, calls=%fused_computation.2 | loop fusion | flops 3145216 | bytes 2099200 | tf_op jit(solution)/shard_map/reduce_sum | solution.py:142
  5.3 2.1 %fusion.2 = bf16[512,2048]{1,0:T(8,128)(2,1)S(1)} fusion(bf16[512,2048]{1,0:T(8,128)(2,1)} %param.20, f32[2048]{0:T(1024)S(1)} %copy-done.8, f32[512]{0:T(512)S(1)} %add_rsqrt_fusion), kind=kLoop, calls=%fused_computation.4 | loop fusion | flops 4194304 | bytes 4204544 | tf_op jit(solution)/shard_map/convert_element_type | solution.py:143
  8.8 2.0 %convolution_convert_fusion.1 = bf16[512,2048]{1,0:T(8,128)(2,1)} fusion(bf16[512,2048]{1,0:T(8,128)(2,1)S(1)} %fusion.2, s32[]{:T(128)S(6)} %select_n.56, s32[128]{0:T(128)S(1)} %get-tuple-element.3, s32[128]{0:T(128)S(1)} %get-tuple-element.2), kind=kOutput, calls=%fused_computation.6 | convolution fusion | flops 269680640 | bytes 2622468 | tf_op jit(solution)/shard_map/dot_general | solution.py:65
  10.8 7.4 %all-to-all-start = ((bf16[8,64,2048]{2,1,0:T(8,128)(2,1)}), bf16[8,64,2048]{2,1,0:T(8,128)(2,1)}, u32[]{:S(2)}, u32[]{:S(2)}) async-start(bf16[8,64,2048]{2,1,0:T(8,128)(2,1)} %bitcast.69), calls=%async_computation | async-start | bytes 4194304 | tf_op jit(solution)/shard_map/all_to_all | solution.py:162
  18.2 1.6 collective-permute-start.5
  22.6 3.9 %collective-permute-start = (bf16[2,2,512]{2,1,0:T(2,128)(2,1)S(1)}, bf16[2,2,512]{2,1,0:T(2,128)(2,1)S(1)}, u32[]{:S(2)}, u32[]{:S(2)}) collective-permute-start(bf16[2,2,512]{2,1,0:T(2,128)(2,1)S(1)} %pad_maximum_fusion.1), channel_id=1, source_target_pairs={{0,4},{4,8},{8,12},{12,16},{16,20},{20,24},{24,28},{1,5},{5,9},{9,... | collective-permute-start | bytes 12296 | tf_op jit(solution)/shard_map/ppermute | solution.py:12
  26.4 8.9 %collective-permute-done = bf16[2,2,512]{2,1,0:T(2,128)(2,1)S(1)} collective-permute-done((bf16[2,2,512]{2,1,0:T(2,128)(2,1)S(1)}, bf16[2,2,512]{2,1,0:T(2,128)(2,1)S(1)}, u32[]{:S(2)}, u32[]{:S(2)}) %collective-permute-start) | collective-permute-done | bytes 4128 | tf_op jit(solution)/shard_map/ppermute | solution.py:12
  35.4 9.1 %collective-permute-done.5 = bf16[1,2048,256]{2,1,0:T(8,128)(2,1)} collective-permute-done((bf16[1,2048,256]{2,1,0:T(8,128)(2,1)S(1)}, bf16[1,2048,256]{2,1,0:T(8,128)(2,1)}, u32[]{:S(2)}, u32[]{:S(2)}) %collective-permute-start.5) | collective-permute-done | bytes 1048608 | tf_op jit(solution)/shard_map/ppermute | solution.py:17
  44.4 22.5 %collective-permute-done.8 = bf16[1,2048,256]{2,1,0:T(8,128)(2,1)} collective-permute-done((bf16[1,2048,256]{2,1,0:T(8,128)(2,1)}, bf16[1,2048,256]{2,1,0:T(8,128)(2,1)}, u32[]{:S(2)}, u32[]{:S(2)}) %collective-permute-start.8) | collective-permute-done | bytes 1048608 | tf_op jit(solution)/shard_map/ppermute | solution.py:17
  66.9 21.0 %collective-permute-done.11 = bf16[1,256,2048]{2,1,0:T(8,128)(2,1)} collective-permute-done((bf16[1,256,2048]{2,1,0:T(8,128)(2,1)}, bf16[1,256,2048]{2,1,0:T(8,128)(2,1)}, u32[]{:S(2)}, u32[]{:S(2)}) %collective-permute-start.11) | collective-permute-done | bytes 1048608 | tf_op jit(solution)/shard_map/ppermute | solution.py:17
  89.1 2.5 %convert_multiply_fusion.2 = f32[512,512]{1,0:T(8,128)} fusion(bf16[512,512]{1,0:T(8,128)(2,1)} %param.15, bf16[512,512]{1,0:T(8,128)(2,1)} %param.16), kind=kLoop, calls=%fused_computation.32 | loop fusion | flops 786432 | bytes 2097152 | tf_op jit(solution)/shard_map/mul | solution.py:124
  91.6 2.7 %fusion.41 = f32[512,256]{1,0:T(8,128)} fusion(bf16[512,2048]{1,0:T(8,128)(2,1)S(1)} %copy-done.2, bf16[2048,256]{1,0:T(8,128)(2,1)} %param.27), kind=kOutput, calls=%fused_computation.81 | convolution fusion | flops 536870912 | bytes 3670016 | tf_op jit(solution)/shard_map/dot_general | solution.py:145
  95.4 13.2 %shard_map.158 = bf16[512,2048]{1,0:T(8,128)(2,1)} custom-call(bf16[512,2048]{1,0:T(8,128)(2,1)} %bitcast.18.refs_0_, bf16[2048,256]{1,0:T(8,128)(2,1)} %bitcast.75, bf16[2048,256]{1,0:T(8,128)(2,1)} %bitcast.20.refs_2_, bf16[2048,256]{1,0:T(8,128)(2,1)} %bitcast.21.refs_3_, bf16[2048,256]{1,0:T(8,128)(2,1)} %bitcast.22.refs_4_, bf16[2048,256]{1,0:T(8,128)(2,1)} %bitcast.76, ...), custom_call_target="tpu_custom_call" | custom-call | tf_op jit(solution)/shard_map/pallas_call | solution.py:83
  108.6 5.8 %all-to-all-start.1 = ((bf16[8,64,2048]{2,1,0:T(8,128)(2,1)}), bf16[8,64,2048]{2,1,0:T(8,128)(2,1)}, u32[]{:S(2)}, u32[]{:S(2)}) async-start(bf16[8,64,2048]{2,1,0:T(8,128)(2,1)} %bitcast.70), calls=%async_computation.1 | async-start | bytes 4194304 | tf_op jit(solution)/shard_map/all_to_all | solution.py:184
  114.4 2.5 %convolution_convert_fusion.2 = bf16[512,2048]{1,0:T(8,128)(2,1)S(1)} fusion(bf16[512,2048]{1,0:T(8,128)(2,1)S(1)} %copy-done, f32[2,512]{1,0:T(2,128)S(1)} %multiply_bitcast_fusion, f32[512,512]{1,0:T(8,128)S(1)} %copy-done.7, bf16[512,512]{1,0:T(8,128)(2,1)} %param.17, f32[512]{0:T(512)S(1)} %bitcast.80, f32[512]{0:T(512)S(1)} %bitcast.81, f32[512]{0:T(512)S(1)} %bitcast.79), kind=kOutput, calls=%fused_computation.7 | convolution fusion | flops 1077411840 | bytes 5777408 | tf_op jit(solution)/shard_map/dot_general | solution.py:132
  119.3 5.7 %convolution_convert_fusion = bf16[512,2048]{1,0:T(8,128)(2,1)} fusion(bf16[256,2048]{1,0:T(8,128)(2,1)S(1)} %copy-done.10, bf16[512,2048]{1,0:T(8,128)(2,1)} %copy-done.1, bf16[2048,256]{1,0:T(8,128)(2,1)} %param.28, f32[512,256]{1,0:T(8,128)} %fusion.41), kind=kOutput, calls=%fused_computation.5 | convolution fusion | flops 1075576832 | bytes 6815744 | tf_op jit(solution)/shard_map/dot_general | solution.py:148
  127.0 2.1 %fusion.4 = bf16[2,128,2048]{2,1,0:T(8,128)(2,1)S(1)} fusion(bf16[2,128,2048]{2,1,0:T(8,128)(2,1)} %collective-permute-done.1, bf16[2,2,128,2048]{3,2,1,0:T(8,128)(2,1)} %bitcast.74, s32[]{:T(128)S(6)} %select_n.50), kind=kLoop, calls=%fused_computation.13 | loop fusion | flops 2097152 | bytes 3145732 | tf_op jit(solution)/shard_map/convert_element_type | solution.py:51
  129.1 1.6 collective-permute-start.2
  130.7 1.6 fusion.3
  133.7 10.3 %collective-permute-done.2 = bf16[1,128,2048]{2,1,0:T(8,128)(2,1)S(1)} collective-permute-done((bf16[1,128,2048]{2,1,0:T(8,128)(2,1)S(1)}, bf16[1,128,2048]{2,1,0:T(8,128)(2,1)S(1)}, u32[]{:S(2)}, u32[]{:S(2)}) %collective-permute-start.2) | collective-permute-done | bytes 524320 | tf_op jit(solution)/shard_map/ppermute | solution.py:17
  144.9 18.0 %all-to-all-done.1 = bf16[8,64,2048]{2,1,0:T(8,128)(2,1)} async-done(((bf16[8,64,2048]{2,1,0:T(8,128)(2,1)}), bf16[8,64,2048]{2,1,0:T(8,128)(2,1)}, u32[]{:S(2)}, u32[]{:S(2)}) %all-to-all-start.1) | async-done | bytes 2097184 | tf_op jit(solution)/shard_map/all_to_all | solution.py:184
  162.9 2.1 %convolution_multiply_fusion = f32[128,2048]{1,0:T(8,128)S(1)} fusion(bf16[512,2048]{1,0:T(8,128)(2,1)} %bitcast.32, f32[128]{0:T(128)S(1)} %get-tuple-element.8, s32[128]{0:T(128)S(1)} %get-tuple-element.3), kind=kOutput, calls=%fused_computation.8 | convolution fusion | flops 268763136 | bytes 3146752 | tf_op jit(solution)/shard_map/dot_general | solution.py:65
  165.0 2.1 %convolution_multiply_fusion.1 = f32[128,2048]{1,0:T(8,128)S(1)} fusion(bf16[512,2048]{1,0:T(8,128)(2,1)} %bitcast.32, f32[128]{0:T(128)S(1)} %get-tuple-element.7, s32[128]{0:T(128)S(1)} %get-tuple-element.2), kind=kOutput, calls=%fused_computation.9 | convolution fusion | flops 268763136 | bytes 3146752 | tf_op jit(solution)/shard_map/dot_general | solution.py:65
  167.1 2.1 %fusion.14 = bf16[128,2048]{1,0:T(8,128)(2,1)} fusion(f32[128,2048]{1,0:T(8,128)S(1)} %convolution_multiply_fusion, f32[128,2048]{1,0:T(8,128)S(1)} %convolution_multiply_fusion.1, bf16[1,128,2048]{2,1,0:T(8,128)(2,1)} %collective-permute-done.4, bf16[2,128,2048]{2,1,0:T(8,128)(2,1)S(1)} %fusion.3, s32[]{:T(128)S(6)} %select_n.54), kind=kLoop, calls=%fused_computation.28 | loop fusion | flops 1572864 | bytes 3670020 | tf_op jit(solution)/shard_map/convert_element_type | solution.py:192
  (70 shorter events, 15.5 us)
Async XLA Ops:
  0.6 113.8 %copy-start = (bf16[512,2048]{1,0:T(8,128)(2,1)S(1)}, bf16[512,2048]{1,0:T(8,128)(2,1)}, u32[]{:S(2)}) copy-start(bf16[512,2048]{1,0:T(8,128)(2,1)} %param.19) | copy-start | bytes 6291460
  0.6 4.6 %copy-start.8 = (f32[2048]{0:T(1024)S(1)}, f32[2048]{0:T(1024)}, u32[]{:S(2)}) copy-start(f32[2048]{0:T(1024)} %param.21) | copy-start | bytes 24580
  10.8 7.4 %copy-start.5 = (bf16[1,2048,256]{2,1,0:T(8,128)(2,1)S(1)}, bf16[1,2048,256]{2,1,0:T(8,128)(2,1)}, u32[]{:S(2)}) copy-start(bf16[1,2048,256]{2,1,0:T(8,128)(2,1)} %param.24) | copy-start | bytes 3145732
  10.8 83.7 %all-to-all-start = ((bf16[8,64,2048]{2,1,0:T(8,128)(2,1)}), bf16[8,64,2048]{2,1,0:T(8,128)(2,1)}, u32[]{:S(2)}, u32[]{:S(2)}) async-start(bf16[8,64,2048]{2,1,0:T(8,128)(2,1)} %bitcast.69), calls=%async_computation | async-start | bytes 4194304 | tf_op jit(solution)/shard_map/all_to_all | solution.py:162
  18.2 26.2 %collective-permute-start.5 = (bf16[1,2048,256]{2,1,0:T(8,128)(2,1)S(1)}, bf16[1,2048,256]{2,1,0:T(8,128)(2,1)}, u32[]{:S(2)}, u32[]{:S(2)}) collective-permute-start(bf16[1,2048,256]{2,1,0:T(8,128)(2,1)S(1)} %copy-done.5), channel_id=1, source_target_pairs={{0,2},{1,3},{2,0},{3,1},{4,6},{5,7},{6,4},{7,5},{8,10},{9,11},{10,... | collective-permute-start | bytes 3145736 | tf_op jit(solution)/shard_map/ppermute | solution.py:17
  19.8 47.1 %collective-permute-start.8 = (bf16[1,2048,256]{2,1,0:T(8,128)(2,1)}, bf16[1,2048,256]{2,1,0:T(8,128)(2,1)}, u32[]{:S(2)}, u32[]{:S(2)}) collective-permute-start(bf16[1,2048,256]{2,1,0:T(8,128)(2,1)} %param.25), channel_id=1, source_target_pairs={{0,2},{1,3},{2,0},{3,1},{4,6},{5,7},{6,4},{7,5},{8,10},{9,11},{10,... | collective-permute-start | bytes 3145736 | tf_op jit(solution)/shard_map/ppermute | solution.py:17
  20.3 67.6 %collective-permute-start.11 = (bf16[1,256,2048]{2,1,0:T(8,128)(2,1)}, bf16[1,256,2048]{2,1,0:T(8,128)(2,1)}, u32[]{:S(2)}, u32[]{:S(2)}) collective-permute-start(bf16[1,256,2048]{2,1,0:T(8,128)(2,1)} %param.26), channel_id=1, source_target_pairs={{0,2},{1,3},{2,0},{3,1},{4,6},{5,7},{6,4},{7,5},{8,10},{9,11},{10,... | collective-permute-start | bytes 3145736 | tf_op jit(solution)/shard_map/ppermute | solution.py:17
  21.8 66.1 %collective-permute-start.6 = (bf16[1,2048,256]{2,1,0:T(8,128)(2,1)S(1)}, bf16[1,2048,256]{2,1,0:T(8,128)(2,1)}, u32[]{:S(2)}, u32[]{:S(2)}) collective-permute-start(bf16[1,2048,256]{2,1,0:T(8,128)(2,1)S(1)} %copy-done.5), channel_id=1, source_target_pairs={{0,1},{1,0},{2,3},{3,2},{4,5},{5,4},{6,7},{7,6},{8,9},{9,8},{10,11... | collective-permute-start | bytes 3145736 | tf_op jit(solution)/shard_map/ppermute | solution.py:17
  22.6 12.8 %collective-permute-start = (bf16[2,2,512]{2,1,0:T(2,128)(2,1)S(1)}, bf16[2,2,512]{2,1,0:T(2,128)(2,1)S(1)}, u32[]{:S(2)}, u32[]{:S(2)}) collective-permute-start(bf16[2,2,512]{2,1,0:T(2,128)(2,1)S(1)} %pad_maximum_fusion.1), channel_id=1, source_target_pairs={{0,4},{4,8},{8,12},{12,16},{16,20},{20,24},{24,28},{1,5},{5,9},{9,... | collective-permute-start | bytes 12296 | tf_op jit(solution)/shard_map/ppermute | solution.py:12
  35.4 59.0 %collective-permute-start.9 = (bf16[1,2048,256]{2,1,0:T(8,128)(2,1)}, bf16[1,2048,256]{2,1,0:T(8,128)(2,1)}, u32[]{:S(2)}, u32[]{:S(2)}) collective-permute-start(bf16[1,2048,256]{2,1,0:T(8,128)(2,1)} %param.25), channel_id=1, source_target_pairs={{0,1},{1,0},{2,3},{3,2},{4,5},{5,4},{6,7},{7,6},{8,9},{9,8},{10,11... | collective-permute-start | bytes 3145736 | tf_op jit(solution)/shard_map/ppermute | solution.py:17
  44.4 50.0 %collective-permute-start.12 = (bf16[1,256,2048]{2,1,0:T(8,128)(2,1)}, bf16[1,256,2048]{2,1,0:T(8,128)(2,1)}, u32[]{:S(2)}, u32[]{:S(2)}) collective-permute-start(bf16[1,256,2048]{2,1,0:T(8,128)(2,1)} %param.26), channel_id=1, source_target_pairs={{0,1},{1,0},{2,3},{3,2},{4,5},{5,4},{6,7},{7,6},{8,9},{9,8},{10,11... | collective-permute-start | bytes 3145736 | tf_op jit(solution)/shard_map/ppermute | solution.py:17
  66.9 27.5 %collective-permute-start.7 = (bf16[1,2048,256]{2,1,0:T(8,128)(2,1)}, bf16[1,2048,256]{2,1,0:T(8,128)(2,1)}, u32[]{:S(2)}, u32[]{:S(2)}) collective-permute-start(bf16[1,2048,256]{2,1,0:T(8,128)(2,1)} %collective-permute-done.5), channel_id=1, source_target_pairs={{0,1},{1,0},{2,3},{3,2},{4,5},{5,4},{6,7},{7,6},{8,9},{9,8},{10,11... | collective-permute-start | bytes 3145736 | tf_op jit(solution)/shard_map/ppermute | solution.py:17
  87.9 6.5 %collective-permute-start.10 = (bf16[1,2048,256]{2,1,0:T(8,128)(2,1)}, bf16[1,2048,256]{2,1,0:T(8,128)(2,1)}, u32[]{:S(2)}, u32[]{:S(2)}) collective-permute-start(bf16[1,2048,256]{2,1,0:T(8,128)(2,1)} %collective-permute-done.8), channel_id=1, source_target_pairs={{0,1},{1,0},{2,3},{3,2},{4,5},{5,4},{6,7},{7,6},{8,9},{9,8},{10,11... | collective-permute-start | bytes 3145736 | tf_op jit(solution)/shard_map/ppermute | solution.py:17
  87.9 6.5 %collective-permute-start.13 = (bf16[1,256,2048]{2,1,0:T(8,128)(2,1)}, bf16[1,256,2048]{2,1,0:T(8,128)(2,1)S(1)}, u32[]{:S(2)}, u32[]{:S(2)}) collective-permute-start(bf16[1,256,2048]{2,1,0:T(8,128)(2,1)} %collective-permute-done.11), channel_id=1, source_target_pairs={{0,1},{1,0},{2,3},{3,2},{4,5},{5,4},{6,7},{7,6},{8,9},{9,8},{10,11... | collective-permute-start | bytes 3145736 | tf_op jit(solution)/shard_map/ppermute | solution.py:17
  89.1 2.5 %copy-start.2 = (bf16[512,2048]{1,0:T(8,128)(2,1)S(1)}, bf16[512,2048]{1,0:T(8,128)(2,1)}, u32[]{:S(2)}) copy-start(bf16[512,2048]{1,0:T(8,128)(2,1)} %copy-done.1) | copy-start | bytes 6291460
  108.6 5.8 %copy-start.7 = (f32[512,512]{1,0:T(8,128)S(1)}, f32[512,512]{1,0:T(8,128)}, u32[]{:S(2)}) copy-start(f32[512,512]{1,0:T(8,128)} %convert_multiply_fusion.2) | copy-start | bytes 3145732
  108.6 54.3 %all-to-all-start.1 = ((bf16[8,64,2048]{2,1,0:T(8,128)(2,1)}), bf16[8,64,2048]{2,1,0:T(8,128)(2,1)}, u32[]{:S(2)}, u32[]{:S(2)}) async-start(bf16[8,64,2048]{2,1,0:T(8,128)(2,1)} %bitcast.70), calls=%async_computation.1 | async-start | bytes 4194304 | tf_op jit(solution)/shard_map/all_to_all | solution.py:184
  116.9 2.4 %copy-start.10 = (bf16[256,2048]{1,0:T(8,128)(2,1)S(1)}, bf16[256,2048]{1,0:T(8,128)(2,1)}, u32[]{:S(2)}) copy-start(bf16[256,2048]{1,0:T(8,128)(2,1)} %param.29) | copy-start | bytes 3145732
  119.3 7.7 %collective-permute-start.1 = (bf16[2,128,2048]{2,1,0:T(8,128)(2,1)}, bf16[2,128,2048]{2,1,0:T(8,128)(2,1)}, u32[]{:S(2)}, u32[]{:S(2)}) collective-permute-start(bf16[2,128,2048]{2,1,0:T(8,128)(2,1)} %dynamic-slice_bitcast_fusion.1), channel_id=1, source_target_pairs={{0,1},{1,0},{2,3},{3,2},{4,5},{5,4},{6,7},{7,6},{8,9},{9,8},{10,11... | collective-permute-start | bytes 3145736 | tf_op jit(solution)/shard_map/ppermute | solution.py:17
  125.0 1.9 %copy-start.9 = (f32[512,2]{0,1:T(2,128)S(1)}, f32[512,2]{0,1:T(2,128)}, u32[]{:S(2)}) copy-start(f32[512,2]{0,1:T(2,128)} %param.23) | copy-start | bytes 12292
  126.3 4.4 %collective-permute-start.3 = (bf16[2,128,2048]{2,1,0:T(8,128)(2,1)S(1)}, bf16[2,128,2048]{2,1,0:T(8,128)(2,1)}, u32[]{:S(2)}, u32[]{:S(2)}) collective-permute-start(bf16[2,128,2048]{2,1,0:T(8,128)(2,1)S(1)} %dynamic-slice_bitcast_fusion), channel_id=1, source_target_pairs={{0,1},{1,0},{2,3},{3,2},{4,5},{5,4},{6,7},{7,6},{8,9},{9,8},{10,11... | collective-permute-start | bytes 3145736 | tf_op jit(solution)/shard_map/ppermute | solution.py:17
  126.9 3.8 %copy-start.3 = (bf16[512,2048]{1,0:T(8,128)(2,1)S(1)}, bf16[512,2048]{1,0:T(8,128)(2,1)}, u32[]{:S(2)}) copy-start(bf16[512,2048]{1,0:T(8,128)(2,1)} %convolution_convert_fusion) | copy-start | bytes 6291460
  129.1 14.9 %collective-permute-start.2 = (bf16[1,128,2048]{2,1,0:T(8,128)(2,1)S(1)}, bf16[1,128,2048]{2,1,0:T(8,128)(2,1)S(1)}, u32[]{:S(2)}, u32[]{:S(2)}) collective-permute-start(bf16[1,128,2048]{2,1,0:T(8,128)(2,1)S(1)} %constant_dynamic-slice_fusion.3), channel_id=1, source_target_pairs={{0,2},{1,3},{2,0},{3,1},{4,6},{5,7},{6,4},{7,5},{8,10},{9,11},{10,... | collective-permute-start | bytes 1572872 | tf_op jit(solution)/shard_map/ppermute | solution.py:17
  133.2 33.9 %collective-permute-start.4 = (bf16[1,128,2048]{2,1,0:T(8,128)(2,1)}, bf16[1,128,2048]{2,1,0:T(8,128)(2,1)}, u32[]{:S(2)}, u32[]{:S(2)}) collective-permute-start(bf16[1,128,2048]{2,1,0:T(8,128)(2,1)} %constant_dynamic-slice_fusion.2), channel_id=1, source_target_pairs={{0,2},{1,3},{2,0},{3,1},{4,6},{5,7},{6,4},{7,5},{8,10},{9,11},{10,... | collective-permute-start | bytes 1572872 | tf_op jit(solution)/shard_map/ppermute | solution.py:17
  (3 other events, 3.7 us)
